TPU v7x, 32 devices: a whole 2x2x4 slice. The times are simulated.
32 devices in a mesh: grp: 2 (over x), ep: 16 (over z, y, core), tp: 1.
Axes of the slice: x: 2, y: 2, z: 4, core: 2. Of those that a mesh axis runs over, the one named last changes fastest.
Arguments:
- tokens: bfloat16 [2048, 1024], P(('grp', 'ep')), parts along dimension 0, may hold values from -6 to 6
- norm_gain: float32 [1024], replicated, may hold values from 0.1 to 1.9
- routes: int32 [2048, 6], P(('grp', 'ep')), parts along dimension 0, may hold values from 0 to 15, all different within a row; in each aligned block of 64 rows (0 to 63, 64 to 127, ...) at most 32 rows name the same one
- gate_weights: float32 [2048, 6], P(('grp', 'ep')), parts along dimension 0, may hold values from 0.1 to 1
- w_gate: bfloat16 [16, 1024, 2048], P('ep', None, 'tp'), may hold values from -0.1875 to 0.1875
- w_up: bfloat16 [16, 1024, 2048], P('ep', None, 'tp'), may hold values from -0.1875 to 0.1875
- w_down: bfloat16 [16, 2048, 1024], P('ep', 'tp'), may hold values from -0.125 to 0.125
Outputs:
- mixed: bfloat16 [2048, 1024], P(('grp', 'ep')), parts along dimension 0
There are 2 independent parts, one for each index of `grp`. A program takes and returns all parts, laid end to end along the dimension named above; an argument that names none is the same for every part. Nothing has to cross between parts.
Inputs may be any that keep to these rules, and one draw needn't show every extreme that they name: `routes`: each row names 6 different experts. Within the rows of one index of ep no expert is named more than 32 times, and in every draw some expert is named exactly 32 times in some index's rows.
All inputs are finite; a program needn't handle non-finite values.
Results may differ from a plain program's by a relative error of at most 0.013.
Values may be sent and summed in bfloat16 or wider, within the bound.
No kernel may reach another device: no remote copies, remote signals or barrier semaphores. Data moves between devices by JAX's collectives and lax.ppermute only.
A program may use at most 64 MiB of HBM per device.

v0:
```python
import jax
import jax.numpy as jnp
from jax import lax
from jax.sharding import PartitionSpec as P


def hidden_rows(rows, w_gate, w_up):
    gate = jnp.dot(rows, w_gate[0], preferred_element_type=jnp.float32)
    up = jnp.dot(rows, w_up[0], preferred_element_type=jnp.float32)
    return (jax.nn.silu(gate) * up).astype(jnp.bfloat16)


def weigh_rows(combine, returned):
    upper = combine.astype(jnp.bfloat16)
    lower = (combine - upper.astype(jnp.float32)).astype(jnp.bfloat16)
    first = jnp.dot(upper, returned, preferred_element_type=jnp.float32)
    return first + jnp.dot(lower, returned, preferred_element_type=jnp.float32)


def shards(tokens, norm_gain, routes, gate_weights, w_gate, w_up, w_down):
    values = tokens.astype(jnp.float32)
    scale = lax.rsqrt(jnp.mean(values * values, axis=-1, keepdims=True) + 1e-06)
    normed = (values * scale * norm_gain).astype(jnp.bfloat16)
    width = tokens.shape[1]
    tok_dev = tokens.shape[0]
    topk = routes.shape[1]
    experts = lax.axis_size("ep")
    capacity = min(tok_dev, max(2, 4 * tok_dev * topk // (3 * experts)))
    expert_ids = jnp.arange(experts, dtype=jnp.int32)
    hits = routes[:, :, None] == expert_ids[None, None, :]
    chosen = jnp.any(hits, axis=1).astype(jnp.int32)
    weight_tok = jnp.sum(jnp.where(hits, gate_weights[:, :, None], 0.0), axis=1)
    rank = jnp.cumsum(chosen, axis=0) - chosen
    slot = jnp.where(chosen > 0, rank * experts + expert_ids[None, :], -1)
    slot_ids = jnp.arange(capacity * experts, dtype=jnp.int32)
    placed = slot[:, :, None] == slot_ids[None, None, :]
    place = jnp.any(placed, axis=1).astype(jnp.bfloat16)
    combine = jnp.sum(jnp.where(placed, weight_tok[:, :, None], 0.0), axis=1)
    dispatch = jnp.dot(place.T, normed, preferred_element_type=jnp.float32)
    dispatch = dispatch.astype(jnp.bfloat16).reshape(capacity, experts, width)
    arrived = lax.all_to_all(dispatch, "ep", split_axis=1, concat_axis=1, tiled=True)
    rows = arrived.reshape(-1, width)
    partial_value = jnp.dot(
        hidden_rows(rows, w_gate, w_up), w_down[0], preferred_element_type=jnp.float32
    )
    output = lax.psum(partial_value.astype(jnp.bfloat16), "tp")
    returned = lax.all_to_all(
        output.reshape(arrived.shape), "ep", split_axis=1, concat_axis=1, tiled=True
    )
    mixed = weigh_rows(combine, returned.reshape(-1, width))
    return mixed.astype(jnp.bfloat16)


def solution(mesh):
    in_specs = (
        P(("grp", "ep"), None),
        P(),
        P(("grp", "ep"), None),
        P(("grp", "ep"), None),
        P("ep", None, "tp"),
        P("ep", None, "tp"),
        P("ep", "tp", None),
    )
    out_specs = P(("grp", "ep"), None)
    return jax.shard_map(shards, mesh=mesh, in_specs=in_specs, out_specs=out_specs, check_vma=False)
```

profile of v0, /device:TPU:0, one launch (start us, length us, event | category | flops | bytes accessed | tf_op | source)
XLA Modules:
  0.0 82.2 jit_solution(14729144316334113847)
XLA Ops:
  0.0 0.7 fusion.23
  0.7 0.1 copy.20
  0.8 0.1 reduce_window_sum.11
  0.9 0.0 copy-start.2
  0.9 0.5 fusion.8
  1.5 1.3 %fusion.17 = f32[64]{0:T(128)S(1)} fusion(bf16[64,1024]{1,0:T(8,128)(2,1)} %param.7), kind=kLoop, calls=%fused_computation.16 | loop fusion | flops 196544 | bytes 131328 | tf_op jit(solution)/shard_map/reduce_sum | solution.py:22
  2.8 1.4 %convolution_convert_fusion = bf16[512,1024]{1,0:T(8,128)(2,1)S(1)} fusion(pred[64,512]{1,0:T(8,128)(4,1)S(1)} %fusion.8, bf16[64,1024]{1,0:T(8,128)(2,1)} %param.7, f32[1024]{0:T(1024)} %param.8, f32[64]{0:T(128)S(1)} %add_rsqrt_fusion), kind=kOutput, calls=%fused_computation.10 | convolution fusion | flops 67895296 | bytes 1216768 | tf_op jit(solution)/shard_map/dot_general | solution.py:39
  4.2 0.6 copy.22
  4.8 31.9 %all_to_all.10 = bf16[32,16,1024]{2,0,1:T(8,128)(2,1)S(1)} all-to-all(bf16[32,16,1024]{2,0,1:T(8,128)(2,1)S(1)} %copy.22), channel_id=1, replica_groups=mesh['grp'=2,'ep'=16,'tp'=1] {'ep'}, dimensions={1} | all-to-all | bytes 2097152 | tf_op jit(solution)/shard_map/all_to_all | solution.py:41
  36.7 0.6 copy.23
  37.3 0.0 copy-done.2
  37.3 4.3 %fusion.4 = f32[512,2048]{1,0:T(8,128)} fusion(bf16[512,1024]{1,0:T(8,128)(2,1)S(1)} %bitcast.29, bf16[1,1024,2048]{2,1,0:T(8,128)(2,1)S(1)} %copy-done.2), kind=kOutput, calls=%fused_computation.4 | convolution fusion | flops 2147483648 | bytes 9437184 | tf_op jit(solution)/shard_map/dot_general | solution.py:8
  41.6 9.2 %fusion.11 = bf16[512,1024]{1,0:T(8,128)(2,1)S(1)} fusion(bf16[1,2048,1024]{2,1,0:T(8,128)(2,1)} %param.13, f32[512,2048]{1,0:T(8,128)} %fusion.4, bf16[512,1024]{1,0:T(8,128)(2,1)S(1)} %bitcast.30, bf16[1,1024,2048]{2,1,0:T(8,128)(2,1)} %param.12), kind=kOutput, calls=%fused_computation.11 | convolution fusion | flops 4301783040 | bytes 14680064 | tf_op jit(solution)/shard_map/dot_general | solution.py:43
  50.8 0.0 copy-start
  50.8 0.0 copy-start.1
  50.8 1.6 %copy.24 = bf16[32,16,1024]{2,0,1:T(8,128)(2,1)} copy(bf16[32,16,1024]{2,1,0:T(8,128)(2,1)S(1)} %bitcast.31) | data formatting | bytes 2097152 | tf_op jit(solution)/shard_map/reshape | solution.py:48
  52.4 5.0 %all-to-all-start.1 = ((bf16[32,16,1024]{2,0,1:T(8,128)(2,1)}), bf16[32,16,1024]{2,0,1:T(8,128)(2,1)S(1)}, u32[]{:S(2)}, u32[]{:S(2)}) async-start(bf16[32,16,1024]{2,0,1:T(8,128)(2,1)} %copy.24), calls=%async_computation.1 | async-start | bytes 2097152 | tf_op jit(solution)/shard_map/all_to_all | solution.py:47
  57.4 0.0 copy-done
  57.5 0.0 copy-done.1
  57.5 0.1 copy.21
  57.6 0.6 select_reduce_fusion
  58.2 22.1 %all-to-all-done.1 = bf16[32,16,1024]{2,0,1:T(8,128)(2,1)S(1)} async-done(((bf16[32,16,1024]{2,0,1:T(8,128)(2,1)}), bf16[32,16,1024]{2,0,1:T(8,128)(2,1)S(1)}, u32[]{:S(2)}, u32[]{:S(2)}) %all-to-all-start.1) | async-done | bytes 1048608 | tf_op jit(solution)/shard_map/all_to_all | solution.py:47
  80.3 0.6 copy.25
  80.9 0.3 fusion.25
  81.2 1.0 %fusion.16 = bf16[64,1024]{1,0:T(8,128)(2,1)} fusion(f32[64,1024]{1,0:T(8,128)S(1)} %fusion.25, bf16[512,1024]{1,0:T(8,128)(2,1)S(1)} %bitcast.27, f32[64,512]{1,0:T(8,128)S(1)} %select_reduce_fusion), kind=kOutput, calls=%fused_computation.13 | convolution fusion | flops 67371008 | bytes 1572864 | tf_op jit(solution)/shard_map/dot_general | solution.py:17
  (4 shorter events, 0.0 us)
Async XLA Ops:
  0.9 36.4 %copy-start.2 = (bf16[1,1024,2048]{2,1,0:T(8,128)(2,1)S(1)}, bf16[1,1024,2048]{2,1,0:T(8,128)(2,1)}, u32[]{:S(2)}) copy-start(bf16[1,1024,2048]{2,1,0:T(8,128)(2,1)} %param.11) | copy-start | bytes 12582916
  50.8 6.6 %copy-start = (s32[64,6]{0,1:T(8,128)S(1)}, s32[64,6]{0,1:T(8,128)}, u32[]{:S(2)}) copy-start(s32[64,6]{0,1:T(8,128)} %param.9) | copy-start | bytes 4612
  50.8 6.6 %copy-start.1 = (f32[64,6]{0,1:T(8,128)S(1)}, f32[64,6]{0,1:T(8,128)}, u32[]{:S(2)}) copy-start(f32[64,6]{0,1:T(8,128)} %param.10) | copy-start | bytes 4612
  52.4 27.9 %all-to-all-start.1 = ((bf16[32,16,1024]{2,0,1:T(8,128)(2,1)}), bf16[32,16,1024]{2,0,1:T(8,128)(2,1)S(1)}, u32[]{:S(2)}, u32[]{:S(2)}) async-start(bf16[32,16,1024]{2,0,1:T(8,128)(2,1)} %copy.24), calls=%async_computation.1 | async-start | bytes 2097152 | tf_op jit(solution)/shard_map/all_to_all | solution.py:47
where the time goes:
time: 83.7 us; the launch traced here: 82.2 us
  blocking collectives  31.9 us (38%)
  waiting for transfers between devices  22.1 us (26%)
  matrix products  16.2 us (19%)
  starting transfers between devices  5.02 us (6%)
  local copies, waits for them, and re-layouts  3.51 us (4%)
  other arithmetic  3.31 us (4%)
    all_to_all x1, blocking collectives, shards(): lax.all_to_all(dispatch, 'ep', split_axis=1, concat_axis=1, tiled=True)  31.9 us
    all_to_all x1, waiting for transfers between devices, shards(): lax.all_to_all(output.reshape(arrived.shape), 'ep', split_axis=1, concat_...  22.1 us
    dot_general x1, matrix products, shards(): jnp.dot(hidden_rows(rows, w_gate, w_up), w_down[0], preferred_element_typ...  9.22 us
    all_to_all x1, starting transfers between devices, shards(): lax.all_to_all(output.reshape(arrived.shape), 'ep', split_axis=1, concat_...  5.02 us
    dot_general x1, matrix products, hidden_rows(): gate = jnp.dot(rows, w_gate[0], preferred_element_type=jnp.float32)  4.3 us
  transfers between devices with their start and end apart: 1, of which 1 were waited for; matrix products, arithmetic and copies ran while one was open for 1% of the time, Pallas kernels for 0%

commit v1 on v0

v1 whole, which is shorter than its diff:
```python
import jax
import jax.numpy as jnp
from jax import lax
from jax.sharding import PartitionSpec as P


def shards(tokens, norm_gain, routes, gate_weights, w_gate, w_up, w_down):
    values = tokens.astype(jnp.float32)
    scale = lax.rsqrt(jnp.mean(values * values, axis=-1, keepdims=True) + 1e-06)
    normed = (values * scale * norm_gain).astype(jnp.bfloat16)
    width = tokens.shape[1]
    tok_dev = tokens.shape[0]
    topk = routes.shape[1]
    experts = lax.axis_size("ep")
    capacity = min(tok_dev, max(2, 4 * tok_dev * topk // (3 * experts)))
    slots = capacity * experts
    me = lax.axis_index("ep")
    all_normed = lax.all_gather(normed, "ep", axis=0, tiled=True)
    hits = routes[:, :, None] == jnp.arange(experts, dtype=jnp.int32)[None, None, :]
    weight_tok = jnp.sum(jnp.where(hits, gate_weights[:, :, None], 0.0), axis=1)
    weights_t = lax.all_to_all(weight_tok.T, "ep", split_axis=0, concat_axis=0, tiled=True)
    chosen = weights_t > 0.0
    lower = (jnp.arange(tok_dev)[:, None] < jnp.arange(tok_dev)[None, :]).astype(jnp.bfloat16)
    rank = jnp.dot(chosen.astype(jnp.bfloat16), lower, preferred_element_type=jnp.float32)
    base = jnp.arange(experts, dtype=jnp.int32)[:, None] * capacity
    slot = jnp.where(chosen, rank.astype(jnp.int32) + base, -1).reshape(1, -1)
    placed = slot == jnp.arange(slots, dtype=jnp.int32)[:, None]
    place = placed.astype(jnp.bfloat16)
    weight = jnp.sum(jnp.where(placed, weights_t.reshape(1, -1), 0.0), axis=1, keepdims=True)
    rows = jnp.dot(place, all_normed, preferred_element_type=jnp.float32).astype(jnp.bfloat16)
    gate = jnp.dot(rows, w_gate[0], preferred_element_type=jnp.float32)
    up = jnp.dot(rows, w_up[0], preferred_element_type=jnp.float32)
    hidden = (jax.nn.silu(gate) * up).astype(jnp.bfloat16)
    output = jnp.dot(hidden, w_down[0], preferred_element_type=jnp.float32).astype(jnp.bfloat16)
    output = lax.psum(output, "tp")
    terms = (output.astype(jnp.float32) * weight).astype(jnp.bfloat16)
    spread = jnp.dot(place.T, terms, preferred_element_type=jnp.float32).astype(jnp.bfloat16)
    return lax.psum_scatter(spread, "ep", scatter_dimension=0, tiled=True)


def solution(mesh):
    in_specs = (
        P(("grp", "ep"), None),
        P(),
        P(("grp", "ep"), None),
        P(("grp", "ep"), None),
        P("ep", None, "tp"),
        P("ep", None, "tp"),
        P("ep", "tp", None),
    )
    out_specs = P(("grp", "ep"), None)
    return jax.shard_map(shards, mesh=mesh, in_specs=in_specs, out_specs=out_specs, check_vma=False)
```

time: 83.7 us -> 141 us (1.68)
  waiting for transfers between devices: 22.1 us -> 94.6 us
  blocking collectives: 31.9 us -> 0 us
  between operations: 0.12 us -> 13.5 us
  matrix products: 16.2 us -> 19.2 us
  local copies, waits for them, and re-layouts: 3.51 us -> 0.72 us
  starting transfers between devices: 5.02 us -> 7.46 us
  other arithmetic: 3.31 us -> 4.95 us
    reduce_scatter x0 -> x1, waiting for transfers between devices: none -> 60.7 us  [shards(): return lax.psum_scatter(spread, 'ep', scatter_dimension=0, tiled=True)]
    all_to_all x1 -> x0, blocking collectives: 31.9 us -> none  [shards(): lax.all_to_all(dispatch, 'ep', split_axis=1, concat_axis=1, tiled=True)]
    all_gather x0 -> x1, waiting for transfers between devices: none -> 27.5 us  [shards(): all_normed = lax.all_gather(normed, 'ep', axis=0, tiled=True)]
    all_to_all x1, waiting for transfers between devices: 22.1 us -> 6.44 us  [shards(): lax.all_to_all(weight_tok.T, 'ep', split_axis=0, concat_axis=0, tiled=True)]
    dot_general x5, matrix products: 16.2 us -> 19.2 us  [the longest x1 9.23 us: shards(): jnp.dot(hidden, w_down[0], preferred_element_type=jnp.float32)]
    all_to_all x1, starting transfers between devices: 5.02 us -> 7.41 us  [shards(): lax.all_to_all(weight_tok.T, 'ep', split_axis=0, concat_axis=0, tiled=True)]
    reshape x2 -> x0, local copies, waits for them, and re-layouts: 2.15 us -> none  [the longest x1 1.57 us: shards(): output.reshape(arrived.shape)]
    convert_element_type x1, other arithmetic: 0.01 us -> 1.67 us  [shards(): normed = (values * scale * norm_gain).astype(jnp.bfloat16)]
  transfers between devices with their start and end apart: 1 -> 3, of which waited for: 1 -> 3; matrix products, arithmetic and copies ran while one was open for 1% -> 2% of each run, Pallas kernels for 0% -> 0%
where the time goes in v1:
time: 141 us; the launch traced here: 140 us
  waiting for transfers between devices  94.6 us (67%)
  matrix products  19.2 us (14%)
  between operations  13.5 us (10%)
  starting transfers between devices  7.46 us (5%)
  other arithmetic  4.95 us (4%)
    reduce_scatter x1, waiting for transfers between devices, shards(): return lax.psum_scatter(spread, 'ep', scatter_dimension=0, tiled=True)  60.7 us
    all_gather x1, waiting for transfers between devices, shards(): all_normed = lax.all_gather(normed, 'ep', axis=0, tiled=True)  27.5 us
    dot_general x1, matrix products, shards(): jnp.dot(hidden, w_down[0], preferred_element_type=jnp.float32)  9.23 us
    all_to_all x1, starting transfers between devices, shards(): lax.all_to_all(weight_tok.T, 'ep', split_axis=0, concat_axis=0, tiled=True)  7.41 us
    all_to_all x1, waiting for transfers between devices, shards(): lax.all_to_all(weight_tok.T, 'ep', split_axis=0, concat_axis=0, tiled=True)  6.44 us
    dot_general x1, matrix products, shards(): gate = jnp.dot(rows, w_gate[0], preferred_element_type=jnp.float32)  4.29 us
    dot_general x1, matrix products, shards(): jnp.dot(place, all_normed, preferred_element_type=jnp.float32)  2.99 us
  transfers between devices with their start and end apart: 3, of which 3 were waited for; matrix products, arithmetic and copies ran while one was open for 2% of the time, Pallas kernels for 0%

profile of v1, /device:TPU:0, one launch (start us, length us, event | category | flops | bytes accessed | tf_op | source)
XLA Modules:
  0.0 140.5 jit_solution(1114677844592831755)
XLA Ops:
  6.5 0.0 all-gather.2.cloned.1.call-start
  6.5 1.0 fusion.27
  7.6 1.7 %fusion.29 = bf16[64,1024]{1,0:T(8,128)(2,1)} fusion(bf16[64,1024]{1,0:T(8,128)(2,1)} %param.7, f32[1024]{0:T(1024)} %param.8, f32[64]{0:T(128)S(1)} %add_rsqrt_fusion), kind=kLoop, calls=%fused_computation.24 | loop fusion | flops 262144 | bytes 266496 | tf_op jit(solution)/shard_map/convert_element_type | solution.py:10
  9.3 0.0 all-gather.2.cloned.1.call-update
  9.3 1.3 select_reduce_fusion.1
  10.6 7.4 %all-to-all-start = ((f32[16,1,64]{2,1,0:T(1,128)}), f32[16,1,64]{2,1,0:T(1,128)S(1)}, u32[]{:S(2)}, u32[]{:S(2)}) async-start(f32[16,1,64]{2,1,0:T(1,128)} %bitcast.2), calls=%async_computation | async-start | bytes 16384 | tf_op jit(solution)/shard_map/all_to_all | solution.py:21
  18.0 0.0 reduce-scatter.2.cloned.1.call-start
  18.1 6.4 %all-to-all-done = f32[16,1,64]{2,1,0:T(1,128)S(1)} async-done(((f32[16,1,64]{2,1,0:T(1,128)}), f32[16,1,64]{2,1,0:T(1,128)S(1)}, u32[]{:S(2)}, u32[]{:S(2)}) %all-to-all-start) | async-done | bytes 4128 | tf_op jit(solution)/shard_map/all_to_all | solution.py:21
  24.5 0.1 fusion.24
  24.6 0.1 eq.31
  24.7 0.6 broadcast.32
  25.2 0.6 reduce.3
  25.9 0.1 broadcast_in_dim.43
  26.0 0.3 select_reduce_fusion
  26.3 27.5 %all-gather.2.cloned.1.call-done = bf16[1024,1024]{1,0:T(8,128)(2,1)} async-done(((bf16[64,1024]{1,0:T(8,128)(2,1)}), bf16[1024,1024]{1,0:T(8,128)(2,1)}) %all-gather.2.cloned.1.call-update) | async-done | bytes 2097168 | tf_op jit(solution)/shard_map/all_gather | solution.py:18
  53.7 0.0 copy-start
  53.7 3.0 %fusion.13 = bf16[512,1024]{1,0:T(8,128)(2,1)S(1)} fusion(bf16[1024,1024]{1,0:T(8,128)(2,1)} %all-gather.2.cloned.1.call-done, s32[1024]{0:T(1024)S(1)} %eq.31), kind=kOutput, calls=%fused_computation.13 | convolution fusion | flops 1074790400 | bytes 3149824 | tf_op jit(solution)/shard_map/dot_general | solution.py:30
  56.7 0.0 copy-done
  56.7 4.3 %fusion.4 = f32[512,2048]{1,0:T(8,128)} fusion(bf16[512,1024]{1,0:T(8,128)(2,1)S(1)} %fusion.13, bf16[1,1024,2048]{2,1,0:T(8,128)(2,1)S(1)} %copy-done), kind=kOutput, calls=%fused_computation.4 | convolution fusion | flops 2147483648 | bytes 9437184 | tf_op jit(solution)/shard_map/dot_general | solution.py:31
  61.0 9.2 %multiply_convert_fusion.1 = bf16[512,1024]{1,0:T(8,128)(2,1)S(1)} fusion(bf16[1,2048,1024]{2,1,0:T(8,128)(2,1)} %param.13, f32[512,2048]{1,0:T(8,128)} %fusion.4, bf16[512,1024]{1,0:T(8,128)(2,1)S(1)} %fusion.13, bf16[1,1024,2048]{2,1,0:T(8,128)(2,1)} %param.12, f32[512]{0:T(512)S(1)} %select_reduce_fusion), kind=kOutput, calls=%fused_computation.7 | convolution fusion | flops 4303355904 | bytes 14682112 | tf_op jit(solution)/shard_map/dot_general | solution.py:34
  70.2 2.7 %fusion.10 = bf16[1024,1024]{1,0:T(8,128)(2,1)} fusion(bf16[512,1024]{1,0:T(8,128)(2,1)S(1)} %multiply_convert_fusion.1, s32[1024]{0:T(1024)S(1)} %eq.31), kind=kOutput, calls=%fused_computation.12 | convolution fusion | flops 1075314688 | bytes 3149824 | tf_op jit(solution)/shard_map/dot_general | solution.py:37
  72.9 0.0 reduce-scatter.2.cloned.1.call-update
  72.9 60.7 %reduce-scatter.2.cloned.1.call-done = bf16[64,1024]{1,0:T(8,128)(2,1)} async-done(((bf16[1024,1024]{1,0:T(8,128)(2,1)}), bf16[64,1024]{1,0:T(8,128)(2,1)}) %reduce-scatter.2.cloned.1.call-update) | async-done | bytes 131088 | tf_op jit(solution)/shard_map/reduce_scatter | solution.py:38
  (2 shorter events, 0.0 us)
Async XLA Ops:
  6.5 47.2 %all-gather.2.cloned.1.call-start = ((), (), s32[]{:S(2)}) async-start(), calls=%async_computation.2 | async-start | bytes 2228224 | tf_op jit(solution)/shard_map/all_gather | solution.py:18
  10.6 13.9 %all-to-all-start = ((f32[16,1,64]{2,1,0:T(1,128)}), f32[16,1,64]{2,1,0:T(1,128)S(1)}, u32[]{:S(2)}, u32[]{:S(2)}) async-start(f32[16,1,64]{2,1,0:T(1,128)} %bitcast.2), calls=%async_computation | async-start | bytes 16384 | tf_op jit(solution)/shard_map/all_to_all | solution.py:21
  18.0 115.6 %reduce-scatter.2.cloned.1.call-start = ((), (), s32[]{:S(2)}) async-start(), calls=%async_computation.3 | async-start | bytes 2228224 | tf_op jit(solution)/shard_map/reduce_scatter | solution.py:38
  53.7 3.0 %copy-start = (bf16[1,1024,2048]{2,1,0:T(8,128)(2,1)S(1)}, bf16[1,1024,2048]{2,1,0:T(8,128)(2,1)}, u32[]{:S(2)}) copy-start(bf16[1,1024,2048]{2,1,0:T(8,128)(2,1)} %param.11) | copy-start | bytes 12582916
Sparse Core Ops, SparseCore 0:
  9.5 44.1 all-gather.1
  73.1 60.5 reduce-scatter.1
